TPU v7x, 32 devices: a whole 2x2x4 slice. The times are simulated.
32 devices in a mesh: sp: 8 (over z, y), dp: 4 (over x, core).
Axes of the slice: x: 2, y: 2, z: 4, core: 2. Of those that a mesh axis runs over, the one named last changes fastest.
Arguments:
- residual: bfloat16 [4, 2048, 2048], P('dp', 'sp'), may hold values from -6 to 6
- queries: bfloat16 [4, 2048, 1024], P('dp', 'sp'), may hold values from -400 to 400
- key_vectors: bfloat16 [4, 2048, 1024], P('dp', 'sp'), may hold values from -6 to 6
- value_vectors: bfloat16 [4, 2048, 1024], P('dp', 'sp'), may hold values from -6 to 6
- gate_cache: float32 [4, 2048, 16], P('dp', 'sp'), may hold values from -258 to 0, as said below
- out_weight: bfloat16 [1024, 2048], P(None, 'dp'), may hold values from -0.1875 to 0.1875
- mix_gain: float32 [2048], replicated, may hold values from 0.1 to 1.9
- route_gain: float32 [2048], replicated, may hold values from 0.1 to 1.9
- out_gain: float32 [2048], replicated, may hold values from 0.1 to 1.9
- routes: int32 [4, 2048, 2], P('dp', 'sp'), may hold values from 0 to 7, all different within a row; in each aligned block of 256 rows (0 to 255, 256 to 511, ..., all dimensions but the last counted through in order) at most 128 rows name the same one
- group_share: float32 [4, 2048], P('dp', 'sp'), may hold values from 0.2 to 1
- expert_share: float32 [4, 2048, 2], P('dp', 'sp'), may hold values from 0.1 to 1
- gate_proj: bfloat16 [8, 2048, 1024], P('sp'), may hold values from -0.125 to 0.125
- up_proj: bfloat16 [8, 2048, 1024], P('sp'), may hold values from -0.125 to 0.125
- down_proj: bfloat16 [8, 1024, 2048], P('sp'), may hold values from -0.1875 to 0.1875
Outputs:
- layer_out: bfloat16 [4, 2048, 2048], P('dp', 'sp')
Inputs may be any that keep to these rules, and one draw needn't show every extreme that they name: `gate_cache`: along the positions of a sequence the values never rise. `routes`: the 2 experts of a position differ. Within the rows of one device (aligned blocks of 256 positions) no expert is named more than 128 times, a bound that some block reaches.
All inputs are finite; a program needn't handle non-finite values.
Results may differ from a plain program's by a relative error of at most 0.0085.
Values may be sent and summed in bfloat16 or wider, within the bound.
A program may use at most 128 MiB of HBM per device.

v0:
```python
import jax
import jax.numpy as jnp
from jax import lax
from jax.sharding import PartitionSpec as P


def normalize(values):
    return values * lax.rsqrt(jnp.mean(values * values, axis=-1, keepdims=True) + 1e-06)


def attend(queries, key_rows, value_rows, cum_gates):
    length = queries.shape[0]
    head_count = cum_gates.shape[1]
    head_width = queries.shape[1] // head_count
    score_scale = head_width ** (-0.5)
    q_heads = queries.reshape(length, head_count, head_width)
    k_heads = key_rows.reshape(length, head_count, head_width)
    v_heads = value_rows.reshape(length, head_count, head_width)
    block_rows = min(512, length)
    outputs = []
    for offset in range(0, length, block_rows):
        stop = offset + block_rows
        scores = (
            jnp.einsum(
                "qhd,khd->hqk",
                q_heads[offset:stop],
                k_heads[:stop],
                preferred_element_type=jnp.float32,
            )
            * score_scale
        )
        bias = cum_gates[offset:stop].T[:, :, None] - cum_gates[:stop].T[:, None, :]
        row_pos = offset + jnp.arange(block_rows, dtype=jnp.int32)[:, None]
        col_pos = jnp.arange(stop, dtype=jnp.int32)[None, :]
        scores = jnp.where(col_pos <= row_pos, scores + bias, -1e30)
        row_max = jnp.max(scores, axis=-1, keepdims=True)
        expo_terms = jnp.exp(scores - row_max)
        probs = (expo_terms / jnp.sum(expo_terms, axis=-1, keepdims=True)).astype(jnp.bfloat16)
        mixing = jnp.einsum(
            "hqk,khd->qhd", probs, v_heads[:stop], preferred_element_type=jnp.float32
        )
        outputs.append(mixing.astype(jnp.bfloat16).reshape(block_rows, head_count * head_width))
    return jnp.concatenate(outputs, axis=0)


def body(
    residual,
    queries,
    key_vectors,
    value_vectors,
    gate_cache,
    out_weight,
    mix_gain,
    route_gain,
    out_gain,
    routes,
    group_share,
    expert_share,
    gate_proj,
    up_proj,
    down_proj,
):
    span_size = lax.axis_size("sp")
    tok_rows = residual.shape[1]
    model_width = residual.shape[2]
    by_heads = (
        lax.all_to_all(queries, "sp", split_axis=2, concat_axis=1, tiled=True),
        lax.all_to_all(key_vectors, "sp", split_axis=2, concat_axis=1, tiled=True),
        lax.all_to_all(value_vectors, "sp", split_axis=2, concat_axis=1, tiled=True),
    )
    cum_gates = lax.all_to_all(gate_cache, "sp", split_axis=2, concat_axis=1, tiled=True)
    attended = attend(by_heads[0][0], by_heads[1][0], by_heads[2][0], cum_gates[0])
    by_tokens = lax.all_to_all(attended[None], "sp", split_axis=1, concat_axis=2, tiled=True)[0]
    mixing = jnp.dot(
        by_tokens,
        lax.all_gather(out_weight, "dp", axis=1, tiled=True),
        preferred_element_type=jnp.float32,
    )
    hidden = (residual[0].astype(jnp.float32) + normalize(mixing) * mix_gain).astype(jnp.bfloat16)
    routed = (normalize(hidden.astype(jnp.float32)) * route_gain).astype(jnp.bfloat16)
    top_count = routes.shape[2]
    experts = span_size * gate_proj.shape[0]
    capacity = 4 * tok_rows // span_size
    assigned = routes[0].reshape(-1)
    expert_ids = jnp.arange(experts, dtype=jnp.int32)
    one_hot = (assigned[:, None] == expert_ids[None, :]).astype(jnp.int32)
    ranking = jnp.sum((jnp.cumsum(one_hot, axis=0) - one_hot) * one_hot, axis=1)
    slot_index = assigned * capacity + ranking
    owners = jnp.arange(assigned.shape[0], dtype=jnp.int32) // top_count
    slot_token = jnp.full((experts * capacity,), tok_rows, jnp.int32).at[slot_index].set(owners)
    padded = jnp.concatenate([routed, jnp.zeros((1, model_width), jnp.bfloat16)], axis=0)
    outgoing = padded[slot_token].reshape(experts, capacity, model_width)
    arrived = lax.all_to_all(outgoing, "sp", split_axis=0, concat_axis=0, tiled=True)
    rows_in = arrived.reshape(-1, model_width)
    gate = jnp.dot(rows_in, gate_proj[0], preferred_element_type=jnp.float32)
    upper = jnp.dot(rows_in, up_proj[0], preferred_element_type=jnp.float32)
    act = (jax.nn.silu(gate) * upper).astype(jnp.bfloat16)
    result = jnp.dot(act, down_proj[0], preferred_element_type=jnp.float32).astype(jnp.bfloat16)
    returned = lax.all_to_all(
        result.reshape(arrived.shape), "sp", split_axis=0, concat_axis=0, tiled=True
    )
    flat_rows = returned.reshape(experts * capacity, model_width)
    gathered = flat_rows[slot_index].reshape(tok_rows, top_count, model_width)
    shares = expert_share[0]
    weights = group_share[0][:, None] * shares / jnp.sum(shares, axis=1, keepdims=True)
    combined = jnp.sum(weights[:, :, None] * gathered.astype(jnp.float32), axis=1)
    layer_out = (hidden.astype(jnp.float32) + combined * out_gain).astype(jnp.bfloat16)
    return layer_out[None]


def solution(mesh):
    placed = (
        P("dp", "sp", None),
        P("dp", "sp", None),
        P("dp", "sp", None),
        P("dp", "sp", None),
        P("dp", "sp", None),
        P(None, "dp"),
        P(),
        P(),
        P(),
        P("dp", "sp", None),
        P("dp", "sp"),
        P("dp", "sp", None),
        P("sp", None, None),
        P("sp", None, None),
        P("sp", None, None),
    )
    return jax.shard_map(
        body, mesh=mesh, in_specs=placed, out_specs=P("dp", "sp", None), check_vma=False
    )
```

profile of v0, /device:TPU:0, one launch (start us, length us, event | category | flops | bytes accessed | tf_op | source)
XLA Modules:
  0.0 412.0 jit_solution(16287597655237337746)
XLA Ops:
  7.9 7.3 %all-to-all-start.2 = ((f32[1,256,16]{1,0,2:T(1,128)}), f32[1,256,16]{1,0,2:T(1,128)S(1)}, u32[]{:S(2)}, u32[]{:S(2)}) async-start(f32[1,256,16]{1,0,2:T(1,128)} %copy.70), calls=%async_computation.2 | async-start | bytes 32768 | tf_op jit(solution)/shard_map/all_to_all | solution.py:71
  18.2 3.9 reduce.5
  23.0 6.0 %all-to-all-start.1 = ((bf16[8,2,16384]{2,1,0:T(2,128)(2,1)}), bf16[8,2,16384]{2,1,0:T(2,128)(2,1)S(1)}, u32[]{:S(2)}, u32[]{:S(2)}) async-start(bf16[8,2,16384]{2,1,0:T(2,128)(2,1)} %reshape.227), calls=%async_computation.1 | async-start | bytes 1048576 | tf_op jit(solution)/shard_map/all_to_all | solution.py:68
  31.4 3.9 reduce.4
  37.1 3.9 reduce.3
  43.0 14.3 %all-to-all-start.3 = ((bf16[8,2,16384]{2,1,0:T(2,128)(2,1)}), bf16[8,2,16384]{2,1,0:T(2,128)(2,1)S(1)}, u32[]{:S(2)}, u32[]{:S(2)}) async-start(bf16[8,2,16384]{2,1,0:T(2,128)(2,1)} %reshape.223), calls=%async_computation.3 | async-start | bytes 1048576 | tf_op jit(solution)/shard_map/all_to_all | solution.py:69
  60.3 10.6 %all-to-all-done.3 = bf16[8,2,16384]{2,1,0:T(2,128)(2,1)S(1)} async-done(((bf16[8,2,16384]{2,1,0:T(2,128)(2,1)}), bf16[8,2,16384]{2,1,0:T(2,128)(2,1)S(1)}, u32[]{:S(2)}, u32[]{:S(2)}) %all-to-all-start.3) | async-done | bytes 524320 | tf_op jit(solution)/shard_map/all_to_all | solution.py:69
  94.7 3.8 fusion.43
  100.9 3.8 fusion.93
  104.8 5.0 %fusion.44 = bf16[2,512,64]{1,2,0:T(8,128)(2,1)S(1)} fusion(bf16[1536,2,64]{0,2,1:T(8,128)(2,1)S(1)} %slice.130, f32[2,512]{1,0:T(2,128)S(1)} %fusion.93, f32[2,1536]{1,0:T(2,128)S(1)} %bitcast.223, f32[2,512]{1,0:T(2,128)} %bitcast.233, pred[512,1536]{1,0:T(8,128)(4,1)} %iota_compare_fusion.1, bf16[512,2,64]{0,2,1:T(8,128)(2,1)} %copy-done.12, ...), kind=kOutput, calls=%fused_computation.65 | convolution fusion | flops 413731328 | bytes 1855488 | tf_op jit(solution)/shard_map/hqk,khd->qhd/dot_general | solution.py:39
  114.5 4.8 %fusion.45 = bf16[2,512,64]{1,2,0:T(8,128)(2,1)S(1)} fusion(bf16[2048,2,64]{0,2,1:T(8,128)(2,1)S(1)} %reshape_squeeze.9, f32[2,512]{1,0:T(2,128)S(1)} %fusion.92, f32[2,2048]{1,0:T(2,128)S(1)} %bitcast.221, f32[2,512]{1,0:T(2,128)} %bitcast.231, pred[512,2048]{1,0:T(8,128)(4,1)S(1)} %copy-done.2, bf16[512,2,64]{0,2,1:T(8,128)(2,1)S(1)} %slice.132, ...), kind=kOutput, calls=%fused_computation.66 | convolution fusion | flops 551619584 | bytes 2383872 | tf_op jit(solution)/shard_map/hqk,khd->qhd/dot_general | solution.py:39
  122.8 8.3 %copy.110 = bf16[1,2048,128]{2,0,1:T(2,128)(2,1)S(1)} copy(bf16[1,2048,128]{2,1,0:T(8,128)(2,1)S(1)} %maximum_bitcast_fusion) | data formatting | bytes 1048576 | tf_op jit(solution)/shard_map/broadcast_in_dim | solution.py:73
  131.1 11.6 %reduce.6 = bf16[2048,128]{1,0:T(8,128)(2,1)S(1)} reduce(bf16[2048,1,128]{2,1,0:T(2,128)(2,1)S(1)} %bitcast.205, bf16[]{:T(256)} %broadcast.162), dimensions={1}, to_apply=%bitcast.187.reduce_sub_computation | reduce | bytes 1048578
  150.5 10.9 %all-to-all-done.4 = bf16[8,2,16384]{2,1,0:T(2,128)(2,1)S(1)} async-done(((bf16[8,2,16384]{2,1,0:T(2,128)(2,1)}), bf16[8,2,16384]{2,1,0:T(2,128)(2,1)S(1)}, u32[]{:S(2)}, u32[]{:S(2)}) %all-to-all-start.4) | async-done | bytes 524320 | tf_op jit(solution)/shard_map/all_to_all | solution.py:73
  167.1 6.0 %gather_fusion = bf16[1024,2048]{1,0:T(8,128)(2,1)} fusion(bf16[257,2048]{1,0:T(8,128)(2,1)S(1)} %concatenate.7, s32[1024]{0:T(1024)S(1)} %fusion.54), kind=kCustom, calls=%fused_computation | custom fusion | bytes 8392704 | tf_op jit(solution)/shard_map/gather | solution.py:92
  173.1 97.0 %all_to_all.85 = bf16[8,128,2048]{2,1,0:T(8,128)(2,1)S(1)} all-to-all(bf16[8,128,2048]{2,1,0:T(8,128)(2,1)} %bitcast.188), channel_id=1, replica_groups=mesh['sp'=8,'dp'=4] {'sp'}, dimensions={0} | all-to-all | bytes 8388608 | tf_op jit(solution)/shard_map/all_to_all | solution.py:93
  270.2 4.5 %fusion.8 = f32[1024,1024]{1,0:T(8,128)S(1)} fusion(bf16[1024,2048]{1,0:T(8,128)(2,1)S(1)} %bitcast.202, bf16[1,2048,1024]{2,1,0:T(8,128)(2,1)S(1)} %copy-done.28), kind=kOutput, calls=%fused_computation.17 | convolution fusion | flops 4294967296 | bytes 12582912 | tf_op jit(solution)/shard_map/dot_general | solution.py:96
  274.7 5.4 %multiply_convert_fusion = bf16[1024,1024]{1,0:T(8,128)(2,1)S(1)} fusion(f32[1024,1024]{1,0:T(8,128)S(1)} %fusion.8, bf16[1024,2048]{1,0:T(8,128)(2,1)S(1)} %bitcast.203, bf16[1,2048,1024]{2,1,0:T(8,128)(2,1)S(1)} %copy-done.29), kind=kOutput, calls=%fused_computation.22 | convolution fusion | flops 4301258752 | bytes 14680064 | tf_op jit(solution)/shard_map/dot_general | solution.py:95
  280.1 6.1 %fusion.18 = bf16[1024,2048]{1,0:T(8,128)(2,1)} fusion(bf16[1024,1024]{1,0:T(8,128)(2,1)S(1)} %multiply_convert_fusion, bf16[1,1024,2048]{2,1,0:T(8,128)(2,1)S(1)} %copy-done.30), kind=kOutput, calls=%fused_computation.33 | convolution fusion | flops 4297064448 | bytes 10485760 | tf_op jit(solution)/shard_map/dot_general | solution.py:98
  286.2 4.9 %all-to-all-start.6 = ((bf16[8,128,2048]{2,1,0:T(8,128)(2,1)}), bf16[8,128,2048]{2,1,0:T(8,128)(2,1)}, u32[]{:S(2)}, u32[]{:S(2)}) async-start(bf16[8,128,2048]{2,1,0:T(8,128)(2,1)} %bitcast.201), calls=%async_computation.6 | async-start | bytes 8388608 | tf_op jit(solution)/shard_map/all_to_all | solution.py:99
  291.3 92.1 %all-to-all-done.6 = bf16[8,128,2048]{2,1,0:T(8,128)(2,1)} async-done(((bf16[8,128,2048]{2,1,0:T(8,128)(2,1)}), bf16[8,128,2048]{2,1,0:T(8,128)(2,1)}, u32[]{:S(2)}, u32[]{:S(2)}) %all-to-all-start.6) | async-done | bytes 4194336 | tf_op jit(solution)/shard_map/all_to_all | solution.py:99
  383.4 7.1 %gather_fusion.1 = bf16[512,2048]{1,0:T(8,128)(2,1)S(1)} fusion(bf16[1024,2048]{1,0:T(8,128)(2,1)} %bitcast.36, s32[1024]{0:T(1024)S(1)} %pad_clamp_fusion), kind=kCustom, calls=%fused_computation.1 | custom fusion | bytes 4196352 | tf_op jit(solution)/shard_map/gather | solution.py:103
  390.5 4.0 reshape.194
  394.5 8.9 %multiply_reduce_fusion = f32[256,2048]{1,0:T(8,128)S(1)} fusion(f32[256,2,2048]{2,1,0:T(2,128)} %reshape.194, f32[256,2]{1,0:T(8,128)S(1)} %copy.90), kind=kLoop, calls=%fused_computation.21 | loop fusion | flops 1572864 | bytes 6293504 | tf_op jit(solution)/shard_map/reduce_sum | solution.py:106
  (173 shorter events, 63.3 us)
Async XLA Ops:
  6.5 23.2 %copy-start.20 = (s32[1,256,2]{1,2,0:T(2,128)S(1)}, s32[1,256,2]{1,2,0:T(2,128)}, u32[]{:S(2)}) copy-start(s32[1,256,2]{1,2,0:T(2,128)} %param.24) | copy-start | bytes 6148
  6.5 24.0 %copy-start.5 = (bf16[1,256,1024]{2,1,0:T(8,128)(2,1)S(1)}, bf16[1,256,1024]{2,1,0:T(8,128)(2,1)}, u32[]{:S(2)}) copy-start(bf16[1,256,1024]{2,1,0:T(8,128)(2,1)} %param.16) | copy-start | bytes 1572868
  7.9 15.1 %all-to-all-start.2 = ((f32[1,256,16]{1,0,2:T(1,128)}), f32[1,256,16]{1,0,2:T(1,128)S(1)}, u32[]{:S(2)}, u32[]{:S(2)}) async-start(f32[1,256,16]{1,0,2:T(1,128)} %copy.70), calls=%async_computation.2 | async-start | bytes 32768 | tf_op jit(solution)/shard_map/all_to_all | solution.py:71
  22.1 14.1 %copy-start.6 = (bf16[1,256,1024]{2,1,0:T(8,128)(2,1)S(1)}, bf16[1,256,1024]{2,1,0:T(8,128)(2,1)}, u32[]{:S(2)}) copy-start(bf16[1,256,1024]{2,1,0:T(8,128)(2,1)} %param.18) | copy-start | bytes 1572868
  23.0 20.0 %all-to-all-start.1 = ((bf16[8,2,16384]{2,1,0:T(2,128)(2,1)}), bf16[8,2,16384]{2,1,0:T(2,128)(2,1)S(1)}, u32[]{:S(2)}, u32[]{:S(2)}) async-start(bf16[8,2,16384]{2,1,0:T(2,128)(2,1)} %reshape.227), calls=%async_computation.1 | async-start | bytes 1048576 | tf_op jit(solution)/shard_map/all_to_all | solution.py:68
  29.0 133.4 %all-gather.2.cloned.1.call-start = ((), (), s32[]{:S(2)}) async-start(), calls=%async_computation.7 | async-start | bytes 5242880 | tf_op jit(solution)/shard_map/all_gather | solution.py:76
  43.0 27.9 %all-to-all-start.3 = ((bf16[8,2,16384]{2,1,0:T(2,128)(2,1)}), bf16[8,2,16384]{2,1,0:T(2,128)(2,1)S(1)}, u32[]{:S(2)}, u32[]{:S(2)}) async-start(bf16[8,2,16384]{2,1,0:T(2,128)(2,1)} %reshape.223), calls=%async_computation.3 | async-start | bytes 1048576 | tf_op jit(solution)/shard_map/all_to_all | solution.py:69
  70.9 17.5 %all-to-all-start = ((bf16[8,2,16384]{2,1,0:T(2,128)(2,1)}), bf16[8,2,16384]{2,1,0:T(2,128)(2,1)S(1)}, u32[]{:S(2)}, u32[]{:S(2)}) async-start(bf16[8,2,16384]{2,1,0:T(2,128)(2,1)} %reshape.225), calls=%async_computation | async-start | bytes 1048576 | tf_op jit(solution)/shard_map/all_to_all | solution.py:67
  104.8 5.4 %copy-start.10 = (bf16[1,2,256,128]{2,3,1,0:T(8,128)(2,1)S(1)}, bf16[1,2,256,128]{2,3,1,0:T(8,128)(2,1)}, u32[]{:S(2)}) copy-start(bf16[1,2,256,128]{2,3,1,0:T(8,128)(2,1)} %get-tuple-element.8) | copy-start | bytes 393220
  104.8 5.9 %copy-start.2 = (pred[512,2048]{1,0:T(8,128)(4,1)S(1)}, pred[512,2048]{1,0:T(8,128)(4,1)}, u32[]{:S(2)}) copy-start(pred[512,2048]{1,0:T(8,128)(4,1)} %iota_compare_fusion) | copy-start | bytes 3145732
  104.8 5.9 %copy-start.13 = (f32[1,2,8,256]{3,1,2,0:T(2,128)S(1)}, f32[1,2,8,256]{3,1,2,0:T(2,128)}, u32[]{:S(2)}) copy-start(f32[1,2,8,256]{3,1,2,0:T(2,128)} %copy.105) | copy-start | bytes 49156
  104.8 5.9 %copy-start.25 = (f32[1,2,2,256]{3,1,2,0:T(2,128)S(1)}, f32[1,2,2,256]{3,1,2,0:T(2,128)}, u32[]{:S(2)}) copy-start(f32[1,2,2,256]{3,1,2,0:T(2,128)} %copy.104) | copy-start | bytes 12292
  114.5 5.0 %copy-start.8 = (bf16[1,2,256,128]{2,3,1,0:T(8,128)(2,1)S(1)}, bf16[1,2,256,128]{2,3,1,0:T(8,128)(2,1)}, u32[]{:S(2)}) copy-start(bf16[1,2,256,128]{2,3,1,0:T(8,128)(2,1)} %get-tuple-element.7) | copy-start | bytes 393220
  114.5 5.2 %copy-start.7 = (bf16[1,2,256,128]{2,3,1,0:T(8,128)(2,1)S(1)}, bf16[1,2,256,128]{2,3,1,0:T(8,128)(2,1)}, u32[]{:S(2)}) copy-start(bf16[1,2,256,128]{2,3,1,0:T(8,128)(2,1)} %slice.143) | copy-start | bytes 393220
  114.5 5.7 %copy-start.11 = (pred[512,512]{0,1:T(8,128)(4,1)S(1)}, pred[512,512]{0,1:T(8,128)(4,1)}, u32[]{:S(2)}) copy-start(pred[512,512]{0,1:T(8,128)(4,1)} %iota_compare_fusion.3) | copy-start | bytes 786436
  114.5 5.7 %copy-start.24 = (f32[1,2,2,256]{3,1,2,0:T(2,128)S(1)}, f32[1,2,2,256]{3,1,2,0:T(2,128)}, u32[]{:S(2)}) copy-start(f32[1,2,2,256]{3,1,2,0:T(2,128)} %copy.99) | copy-start | bytes 12292
  122.6 24.9 %copy-start.1 = (s32[1,256,2]{2,1,0:T(8,128)S(1)}, s32[1,256,2]{2,1,0:T(8,128)}, u32[]{:S(2)}) copy-start(s32[1,256,2]{2,1,0:T(8,128)} %copy-done) | copy-start | bytes 6148
  122.6 25.0 %copy-start.21 = (s32[1,256,2]{1,2,0:T(2,128)S(1)}, s32[1,256,2]{1,2,0:T(2,128)}, u32[]{:S(2)}) copy-start(s32[1,256,2]{1,2,0:T(2,128)} %param.24) | copy-start | bytes 6148
  143.6 17.8 %all-to-all-start.4 = ((bf16[8,2,16384]{2,1,0:T(2,128)(2,1)}), bf16[8,2,16384]{2,1,0:T(2,128)(2,1)S(1)}, u32[]{:S(2)}, u32[]{:S(2)}) async-start(bf16[8,2,16384]{2,1,0:T(2,128)(2,1)} %reshape.229), calls=%async_computation.4 | async-start | bytes 1048576 | tf_op jit(solution)/shard_map/all_to_all | solution.py:73
  173.1 97.0 %copy-start.28 = (bf16[1,2048,1024]{2,1,0:T(8,128)(2,1)S(1)}, bf16[1,2048,1024]{2,1,0:T(8,128)(2,1)}, u32[]{:S(2)}) copy-start(bf16[1,2048,1024]{2,1,0:T(8,128)(2,1)} %param.28) | copy-start | bytes 12582916
  274.7 5.4 %copy-start.30 = (bf16[1,1024,2048]{2,1,0:T(8,128)(2,1)S(1)}, bf16[1,1024,2048]{2,1,0:T(8,128)(2,1)}, u32[]{:S(2)}) copy-start(bf16[1,1024,2048]{2,1,0:T(8,128)(2,1)} %param.29) | copy-start | bytes 12582916
  286.2 5.0 %copy-start.27 = (f32[1,256]{1,0:T(1,128)S(1)}, f32[1,256]{1,0:T(1,128)}, u32[]{:S(2)}) copy-start(f32[1,256]{1,0:T(1,128)} %param.25) | copy-start | bytes 3076
  286.2 97.2 %all-to-all-start.6 = ((bf16[8,128,2048]{2,1,0:T(8,128)(2,1)}), bf16[8,128,2048]{2,1,0:T(8,128)(2,1)}, u32[]{:S(2)}, u32[]{:S(2)}) async-start(bf16[8,128,2048]{2,1,0:T(8,128)(2,1)} %bitcast.201), calls=%async_computation.6 | async-start | bytes 8388608 | tf_op jit(solution)/shard_map/all_to_all | solution.py:99
  394.5 8.9 %copy-start.19 = (f32[2048]{0:T(1024)S(1)}, f32[2048]{0:T(1024)}, u32[]{:S(2)}) copy-start(f32[2048]{0:T(1024)} %param.23) | copy-start | bytes 24580
  (14 other events, 42.1 us)
Sparse Core Ops, SparseCore 0:
  31.4 35.8 all-gather.1
where the time goes:
time: 417 us; the launch traced here: 412 us
  waiting for transfers between devices  118 us (28%)
  blocking collectives  97 us (23%)
  local copies, waits for them, and re-layouts  56 us (13%)
  matrix products  46.1 us (11%)
  other arithmetic  40.6 us (10%)
  starting transfers between devices  39.9 us (10%)
  between operations  14.8 us (4%)
    all_to_all x1, blocking collectives, body(): lax.all_to_all(outgoing, 'sp', split_axis=0, concat_axis=0, tiled=True)  97 us
    all_to_all x1, waiting for transfers between devices, body(): lax.all_to_all(result.reshape(arrived.shape), 'sp', split_axis=0, concat_...  92.1 us
    unnamed x4, other arithmetic  23.1 us
    unnamed x90, local copies, waits for them, and re-layouts  17.4 us
    dot_general x4, matrix products, attend(): jnp.einsum('hqk,khd->qhd', probs, v_heads[:stop], preferred_element_type=...  14.9 us
    all_to_all x1, starting transfers between devices, body(): lax.all_to_all(value_vectors, 'sp', split_axis=2, concat_axis=1, tiled=True)  14.3 us
    sub x4, matrix products, attend(): expo_terms = jnp.exp(scores - row_max)  11.5 us
    all_to_all x1, waiting for transfers between devices, body(): lax.all_to_all(attended[None], 'sp', split_axis=1, concat_axis=2, tiled=T...  10.9 us
  transfers between devices with their start and end apart: 7, of which 5 were waited for; matrix products, arithmetic and copies ran while one was open for 22% of the time, Pallas kernels for 0%

commit v1 on v0

v1 whole, which is shorter than its diff:
```python
import functools
import math
import jax
import jax.numpy as jnp
from jax import lax
from jax.experimental import pallas as pl
from jax.experimental.pallas import tpu as pltpu
from jax.sharding import PartitionSpec as P

LOG2E = math.log2(math.e)
MESH = pl.DeviceIdType.MESH


def normalize(values):
    return values * lax.rsqrt(jnp.mean(values * values, axis=-1, keepdims=True) + 1e-06)


def attend(queries, key_rows, value_rows, cum_gates):
    length = queries.shape[0]
    head_count = cum_gates.shape[1]
    head_width = queries.shape[1] // head_count
    score_scale = head_width ** (-0.5)
    q_heads = queries.reshape(length, head_count, head_width)
    k_heads = key_rows.reshape(length, head_count, head_width)
    v_heads = value_rows.reshape(length, head_count, head_width)
    block_rows = min(512, length)
    outputs = []
    for offset in range(0, length, block_rows):
        stop = offset + block_rows
        scores = (
            jnp.einsum(
                "qhd,khd->hqk",
                q_heads[offset:stop],
                k_heads[:stop],
                preferred_element_type=jnp.float32,
            )
            * score_scale
        )
        bias = cum_gates[offset:stop].T[:, :, None] - cum_gates[:stop].T[:, None, :]
        row_pos = offset + jnp.arange(block_rows, dtype=jnp.int32)[:, None]
        col_pos = jnp.arange(stop, dtype=jnp.int32)[None, :]
        scores = jnp.where(col_pos <= row_pos, scores + bias, -1e30)
        row_max = jnp.max(scores, axis=-1, keepdims=True)
        expo_terms = jnp.exp(scores - row_max)
        probs = (expo_terms / jnp.sum(expo_terms, axis=-1, keepdims=True)).astype(jnp.bfloat16)
        mixing = jnp.einsum(
            "hqk,khd->qhd", probs, v_heads[:stop], preferred_element_type=jnp.float32
        )
        outputs.append(mixing.astype(jnp.bfloat16).reshape(block_rows, head_count * head_width))
    return jnp.concatenate(outputs, axis=0)

def mix_kernel(
    block, heads, span, spread,
    q_in, k_in, v_in, g_in, ow_in, tok_out, ow_out,
    q_all, k_all, v_all, g_all, att, send, recv, back_send, back_recv, ow_send, ow_recv,
):
    me = lax.axis_index("sp")
    mine = lax.axis_index("dp")
    rows = q_in.shape[0]
    width = q_all.shape[1]
    cols = ow_in.shape[1]
    barrier = pltpu.get_barrier_semaphore()
    for d in range(1, span):
        pl.semaphore_signal(barrier, inc=1, device_id={"sp": lax.rem(me + d, span)}, device_id_type=MESH)
    for d in range(1, spread):
        pl.semaphore_signal(barrier, inc=1, device_id={"dp": lax.rem(mine + d, spread)}, device_id_type=MESH)
    pl.semaphore_wait(barrier, span + spread - 2)

    own_rows = pl.ds(pl.multiple_of(me * rows, rows), rows)
    pairs = ((q_in, q_all), (k_in, k_all), (v_in, v_all))
    sends = []
    for d in sorted(range(1, span), key=lambda d: -min(d, span - d)):
        peer = lax.rem(me + d, span)
        lanes = pl.ds(pl.multiple_of(peer * width, width), width)
        for a, (src, dst) in enumerate(pairs):
            sends.append(
                pltpu.make_async_remote_copy(
                    src_ref=src.at[:, lanes], dst_ref=dst.at[own_rows, :],
                    send_sem=send.at[a, d], recv_sem=recv.at[a, me],
                    device_id={"sp": peer}, device_id_type=MESH,
                )
            )
        sends.append(
            pltpu.make_async_remote_copy(
                src_ref=g_in.at[peer], dst_ref=g_all.at[me],
                send_sem=send.at[3, d], recv_sem=recv.at[3, me],
                device_id={"sp": peer}, device_id_type=MESH,
            )
        )
    ow_lanes = pl.ds(pl.multiple_of(mine * cols, cols), cols)
    ow_sends = []
    for d in range(1, spread):
        ow_sends.append(
            pltpu.make_async_remote_copy(
                src_ref=ow_in, dst_ref=ow_out.at[:, ow_lanes],
                send_sem=ow_send.at[d], recv_sem=ow_recv.at[d],
                device_id={"dp": lax.rem(mine + d, spread)}, device_id_type=MESH,
            )
        )
    for copy in sends + ow_sends:
        copy.start()
    own_lanes = pl.ds(pl.multiple_of(me * width, width), width)
    for a, (src, dst) in enumerate(pairs):
        pltpu.make_async_copy(src.at[:, own_lanes], dst.at[own_rows, :], recv.at[a, me]).start()
    pltpu.make_async_copy(g_in.at[me], g_all.at[me], recv.at[3, me]).start()
    ow_local = pltpu.make_async_copy(ow_in, ow_out.at[:, ow_lanes], ow_recv.at[0])
    ow_local.start()

    scale = (width // heads) ** -0.5 * LOG2E
    lane = lax.broadcasted_iota(jnp.int32, (1, width), 1)
    in_head = [(lane // (width // heads)) == h for h in range(heads)]
    row = lax.broadcasted_iota(jnp.int32, (block, block), 0)
    col = lax.broadcasted_iota(jnp.int32, (block, block), 1)
    keep = col <= row
    ones = jnp.ones((block, width), jnp.bfloat16)
    per = block // rows

    def arrive(s):
        at = pl.ds(s * rows, rows)
        for a, (_, dst) in enumerate(pairs):
            pltpu.make_async_copy(dst.at[at, :], dst.at[at, :], recv.at[a, s]).wait()
        pltpu.make_async_copy(g_all.at[s], g_all.at[s], recv.at[3, s]).wait()

    def returned(s):
        return pltpu.make_async_remote_copy(
            src_ref=att.at[pl.ds(s * rows, rows), :], dst_ref=tok_out.at[:, own_lanes],
            send_sem=back_send.at[s], recv_sem=back_recv.at[me],
            device_id={"sp": s}, device_id_type=MESH,
        )

    for i in range(span // per):
        for s in range(i * per, (i + 1) * per):
            arrive(s)
        q = q_all[pl.ds(i * block, block), :]
        outs = []
        for h in range(heads):
            qh = jnp.where(in_head[h], q, jnp.zeros_like(q))
            scores = []
            top = None
            for j in range(i + 1):
                s = lax.dot_general(
                    qh, k_all[pl.ds(j * block, block), :], (((1,), (1,)), ((), ())),
                    preferred_element_type=jnp.float32,
                )
                gate = jnp.concatenate(
                    [g_all[j * per + t, pl.ds(h, 1), :] for t in range(per)], axis=1
                )
                s = s * scale - gate * LOG2E
                if j == i:
                    s = jnp.where(keep, s, -1e30)
                scores.append(s)
                peak = jnp.max(s, axis=1, keepdims=True)
                top = peak if top is None else jnp.maximum(top, peak)
            acc = None
            for j in range(i + 1):
                p = jnp.exp2(scores[j] - top).astype(jnp.bfloat16)
                rhs = jnp.concatenate([v_all[pl.ds(j * block, block), :], ones], axis=1)
                part = jnp.dot(p, rhs, preferred_element_type=jnp.float32)
                acc = part if acc is None else acc + part
            outs.append(acc[:, :width] / acc[:, width:])
        out = outs[0]
        for h in range(1, heads):
            out = jnp.where(in_head[h], outs[h], out)
        att[pl.ds(i * block, block), :] = out.astype(att.dtype)
        for s in range(i * per, (i + 1) * per):
            @pl.when(me != s)
            def _():
                returned(s).start()

            @pl.when(me == s)
            def _():
                pltpu.make_async_copy(
                    att.at[pl.ds(s * rows, rows), :], tok_out.at[:, own_lanes], back_recv.at[s]
                ).start()
    for s in range(span):
        at = pl.ds(s * width, width)
        pltpu.make_async_copy(tok_out.at[:, at], tok_out.at[:, at], back_recv.at[s]).wait()

        @pl.when(me != s)
        def _():
            returned(s).wait_send()
    for copy in sends:
        copy.wait_send()
    ow_local.wait()
    for copy in ow_sends:
        copy.wait()


def mix(queries, keys, values, gates, out_weight, span, spread):
    rows, full = queries.shape
    width = full // span
    heads = gates.shape[1] // span
    per = 2 if span % 2 == 0 else 1
    g = gates.T.reshape(span, heads, rows)
    vm = pl.BlockSpec(memory_space=pltpu.VMEM)
    dma = pltpu.SemaphoreType.DMA
    wide = pltpu.VMEM((span * rows, width), jnp.bfloat16)
    return pl.pallas_call(
        functools.partial(mix_kernel, per * rows, heads, span, spread),
        out_shape=(
            jax.ShapeDtypeStruct((rows, full), jnp.bfloat16),
            jax.ShapeDtypeStruct((full, out_weight.shape[1] * spread), jnp.bfloat16),
        ),
        in_specs=[vm] * 5,
        out_specs=(vm, vm),
        scratch_shapes=[
            wide, wide, wide, pltpu.VMEM((span, heads, rows), jnp.float32), wide,
            dma((4, span)), dma((4, span)), dma((span,)), dma((span,)), dma((spread,)), dma((spread,)),
        ],
        compiler_params=pltpu.CompilerParams(
            collective_id=0, has_side_effects=True, vmem_limit_bytes=50 * 1024 * 1024
        ),
        name="mix",
    )(queries, keys, values, g, out_weight)


def experts_kernel(
    span, chunks,
    routed, pick, weigh, gate_in, up_in, down_in, out,
    w_gate, w_up, w_down, mir, out_own, out_mir, arrived, act, res, back, pbuf, part,
    w_sem, mir_s, mir_r, dir_s, dir_r, two_s, two_r, ret_s, ret_r, rt1_s, rt1_r, part_s, part_r,
):
    half = span // 2
    me = lax.axis_index("sp")
    base = (me // half) * half
    loc = me - base
    mirror = lax.rem(me + half, span)
    cap = arrived.shape[2]
    model = routed.shape[1]
    piece = model // chunks
    ff = act.shape[1]
    partners = [(d, lax.rem(loc + d, half)) for d in range(1, half)]
    barrier = pltpu.get_barrier_semaphore()
    for _, p in partners:
        pl.semaphore_signal(barrier, inc=1, device_id={"sp": base + p}, device_id_type=MESH)
    pl.semaphore_signal(barrier, inc=1, device_id={"sp": mirror}, device_id_type=MESH)
    pl.semaphore_wait(barrier, half)

    def remote(src, dst, s_sem, r_sem, device):
        return pltpu.make_async_remote_copy(
            src_ref=src, dst_ref=dst, send_sem=s_sem, recv_sem=r_sem,
            device_id={"sp": device}, device_id_type=MESH,
        )

    def cols(c):
        return pl.ds(c * piece, piece)

    pending = []

    def begin(copy):
        copy.start()
        pending.append(copy)

    for c in range(chunks):
        begin(remote(routed.at[:, cols(c)], mir.at[:, cols(c)], mir_s.at[c], mir_r.at[c], mirror))
    loads = [
        pltpu.make_async_copy(src, dst, w_sem.at[i])
        for i, (src, dst) in enumerate(((gate_in, w_gate), (up_in, w_up), (down_in, w_down)))
    ]
    for load in loads:
        load.start()

    def rows_of(p):
        return pl.ds(pl.multiple_of(p * cap, cap), cap)

    for d, p in partners:
        chosen = pick[0, rows_of(p), :]
        for c in range(chunks):
            out_own[p, :, cols(c)] = jnp.dot(
                chosen, routed[:, cols(c)], preferred_element_type=jnp.float32
            ).astype(jnp.bfloat16)
        begin(remote(out_own.at[p], arrived.at[0, loc], dir_s.at[d], dir_r.at[loc], base + p))
    chosen = pick[0, rows_of(loc), :]
    for c in range(chunks):
        arrived[0, loc, :, cols(c)] = jnp.dot(
            chosen, routed[:, cols(c)], preferred_element_type=jnp.float32
        ).astype(jnp.bfloat16)

    for c in range(chunks):
        remote(mir.at[:, cols(c)], mir.at[:, cols(c)], mir_s.at[c], mir_r.at[c], mirror).wait_recv()
        for d, p in partners:
            out_mir[p, :, cols(c)] = jnp.dot(
                pick[1, rows_of(p), :], mir[:, cols(c)], preferred_element_type=jnp.float32
            ).astype(jnp.bfloat16)
            begin(
                remote(
                    out_mir.at[p, :, cols(c)], arrived.at[1, loc, :, cols(c)],
                    two_s.at[d, c], two_r.at[loc, c], base + p,
                )
            )
        arrived[1, loc, :, cols(c)] = jnp.dot(
            pick[1, rows_of(loc), :], mir[:, cols(c)], preferred_element_type=jnp.float32
        ).astype(jnp.bfloat16)

    for load in loads:
        load.wait()

    def hidden_units(g):
        tile = math.gcd(256, ff)
        rows_in = arrived.at[g]

        def step(f, carry):
            at = pl.ds(pl.multiple_of(f * tile, tile), tile)
            data = rows_in[...].reshape(half * cap, model)
            gate = jnp.dot(data, w_gate[:, at], preferred_element_type=jnp.float32)
            upper = jnp.dot(data, w_up[:, at], preferred_element_type=jnp.float32)
            act[:, at] = (gate / (1.0 + jnp.exp(-gate)) * upper).astype(jnp.bfloat16)
            return carry

        lax.fori_loop(0, ff // tile, step, 0)

    def results(g, c):
        value = jnp.dot(act[...], w_down[:, cols(c)], preferred_element_type=jnp.float32)
        res[g, :, :, cols(c)] = value.astype(jnp.bfloat16).reshape(half, cap, piece)

    def total(g, c):
        data = back[g, :, :, cols(c)].reshape(half * cap, piece)
        high = jnp.dot(weigh[g, 0], data, preferred_element_type=jnp.float32)
        return high + jnp.dot(weigh[g, 1], data, preferred_element_type=jnp.float32)

    for d, p in partners:
        remote(out_own.at[p], arrived.at[0, p], dir_s.at[d], dir_r.at[p], base + p).wait_recv()
    hidden_units(0)
    for c in range(chunks):
        results(0, c)
    for d, p in partners:
        begin(remote(res.at[0, p], back.at[0, loc], ret_s.at[d], ret_r.at[loc], base + p))
    back[0, loc] = res[0, loc]

    for c in range(chunks):
        for d, p in partners:
            remote(
                out_mir.at[p, :, cols(c)], arrived.at[1, p, :, cols(c)],
                two_s.at[d, c], two_r.at[p, c], base + p,
            ).wait_recv()
    hidden_units(1)
    for c in range(chunks):
        results(1, c)
        for d, p in partners:
            begin(
                remote(
                    res.at[1, p, :, cols(c)], back.at[1, loc, :, cols(c)],
                    rt1_s.at[d, c], rt1_r.at[loc, c], base + p,
                )
            )
        back[1, loc, :, cols(c)] = res[1, loc, :, cols(c)]
    for c in range(chunks):
        for d, p in partners:
            remote(
                res.at[1, p, :, cols(c)], back.at[1, p, :, cols(c)],
                rt1_s.at[d, c], rt1_r.at[p, c], base + p,
            ).wait_recv()
        pbuf[:, cols(c)] = total(1, c).astype(jnp.bfloat16)
        begin(remote(pbuf.at[:, cols(c)], part.at[:, cols(c)], part_s.at[c], part_r.at[c], mirror))
    for d, p in partners:
        remote(res.at[0, p], back.at[0, p], ret_s.at[d], ret_r.at[p], base + p).wait_recv()
    for c in range(chunks):
        own = total(0, c)
        remote(pbuf.at[:, cols(c)], part.at[:, cols(c)], part_s.at[c], part_r.at[c], mirror).wait_recv()
        out[:, cols(c)] = own + part[:, cols(c)].astype(jnp.float32)
    for copy in pending:
        copy.wait_send()


def run_experts(routed, pick, weigh, gate_proj, up_proj, down_proj, span, cap):
    rows, model = routed.shape
    ff = gate_proj.shape[1]
    half = span // 2
    chunks = 4 if model % 512 == 0 else 1
    vm = pl.BlockSpec(memory_space=pltpu.VMEM)
    hbm = pl.BlockSpec(memory_space=pl.ANY)
    dma = pltpu.SemaphoreType.DMA
    bf16 = jnp.bfloat16
    return pl.pallas_call(
        functools.partial(experts_kernel, span, chunks),
        out_shape=jax.ShapeDtypeStruct((rows, model), jnp.float32),
        in_specs=[vm, vm, vm, hbm, hbm, hbm],
        out_specs=vm,
        scratch_shapes=[
            pltpu.VMEM((model, ff), bf16), pltpu.VMEM((model, ff), bf16), pltpu.VMEM((ff, model), bf16),
            pltpu.VMEM((rows, model), bf16),
            pltpu.VMEM((half, cap, model), bf16), pltpu.VMEM((half, cap, model), bf16),
            pltpu.VMEM((2, half, cap, model), bf16),
            pltpu.VMEM((half * cap, ff), bf16),
            pltpu.VMEM((2, half, cap, model), bf16), pltpu.VMEM((2, half, cap, model), bf16),
            pltpu.VMEM((rows, model), bf16), pltpu.VMEM((rows, model), bf16),
            dma((3,)), dma((chunks,)), dma((chunks,)), dma((half,)), dma((half,)),
            dma((half, chunks)), dma((half, chunks)), dma((half,)), dma((half,)),
            dma((half, chunks)), dma((half, chunks)), dma((chunks,)), dma((chunks,)),
        ],
        compiler_params=pltpu.CompilerParams(
            collective_id=1, has_side_effects=True, vmem_limit_bytes=58 * 1024 * 1024
        ),
        name="experts",
    )(routed, pick, weigh, gate_proj, up_proj, down_proj)


def body(
    residual, queries, key_vectors, value_vectors, gate_cache, out_weight, mix_gain, route_gain,
    out_gain, routes, group_share, expert_share, gate_proj, up_proj, down_proj,
):
    span = lax.axis_size("sp")
    spread = lax.axis_size("dp")
    tok_rows = residual.shape[1]
    width = queries.shape[2] // span

    cap = 4 * tok_rows // span
    half = span // 2
    assigned = routes[0].reshape(-1)
    order = jnp.arange(assigned.shape[0], dtype=jnp.int32)
    same = (assigned[:, None] == assigned[None, :]) & (order[None, :] < order[:, None])
    ranking = jnp.sum(same.astype(jnp.int32), axis=1)
    slots = (assigned * cap + ranking).reshape(routes.shape[1:]).astype(jnp.float32)
    shares = expert_share[0]
    weights = group_share[0][:, None] * shares / jnp.sum(shares, axis=1, keepdims=True)
    facts = jnp.stack([slots, weights])
    other = lax.ppermute(facts, "sp", [(i, (i + half) % span) for i in range(span)])
    base = (lax.axis_index("sp") // half) * half
    places = (base * cap + jnp.arange(half * cap, dtype=jnp.int32)).astype(jnp.float32)
    picks, weighs = [], []
    for both in (facts, other):
        hit = both[0][:, :, None] == places[None, None, :]
        picks.append(jnp.any(hit, axis=1).T.astype(jnp.bfloat16))
        high = lax.reduce_precision(both[1], 8, 7)
        weighs.append(
            jnp.stack(
                [jnp.sum(jnp.where(hit, w[:, :, None], 0.0), axis=1) for w in (high, both[1] - high)]
            ).astype(jnp.bfloat16)
        )
    pick, weigh = jnp.stack(picks), jnp.stack(weighs)

    if width % 128 == 0:
        by_tokens, weight_all = mix(
            queries[0], key_vectors[0], value_vectors[0], gate_cache[0], out_weight, span, spread
        )
    else:
        by_heads = [
            lax.all_to_all(x, "sp", split_axis=2, concat_axis=1, tiled=True)
            for x in (queries, key_vectors, value_vectors, gate_cache)
        ]
        attended = attend(*(x[0] for x in by_heads))
        by_tokens = lax.all_to_all(attended[None], "sp", split_axis=1, concat_axis=2, tiled=True)[0]
        weight_all = lax.all_gather(out_weight, "dp", axis=1, tiled=True)
    mixed = jnp.dot(by_tokens, weight_all, preferred_element_type=jnp.float32)
    hidden = (residual[0].astype(jnp.float32) + normalize(mixed) * mix_gain).astype(jnp.bfloat16)
    routed = (normalize(hidden.astype(jnp.float32)) * route_gain).astype(jnp.bfloat16)
    combined = run_experts(routed, pick, weigh, gate_proj[0], up_proj[0], down_proj[0], span, cap)
    layer_out = (hidden.astype(jnp.float32) + combined * out_gain).astype(jnp.bfloat16)
    return layer_out[None]


def solution(mesh):
    placed = (
        P("dp", "sp", None),
        P("dp", "sp", None),
        P("dp", "sp", None),
        P("dp", "sp", None),
        P("dp", "sp", None),
        P(None, "dp"),
        P(),
        P(),
        P(),
        P("dp", "sp", None),
        P("dp", "sp"),
        P("dp", "sp", None),
        P("sp", None, None),
        P("sp", None, None),
        P("sp", None, None),
    )
    return jax.shard_map(
        body, mesh=mesh, in_specs=placed, out_specs=P("dp", "sp", None), check_vma=False
    )
```

time: 417 us -> 234 us (0.56)
  Pallas kernels: 0 us -> 205 us
  waiting for transfers between devices: 118 us -> 0.01 us
  blocking collectives: 97 us -> 0 us
  local copies, waits for them, and re-layouts: 56 us -> 7.02 us
  matrix products: 46.1 us -> 3.61 us
  starting transfers between devices: 39.9 us -> 4.13 us
  other arithmetic: 40.6 us -> 10.5 us
  between operations: 14.8 us -> 0.2 us
    pallas_call x0 -> x2, Pallas kernels: none -> 205 us  [the longest x1 156 us: run_experts(): pl.pallas_call(functools.partial(experts_kernel, span, chunks), out_shape...]
    all_to_all x6 -> x0, waiting for transfers between devices: 117 us -> none  [the longest x1 92.1 us: body(): lax.all_to_all(result.reshape(arrived.shape), 'sp', split_axis=0, concat_...]
    all_to_all x1 -> x0, blocking collectives: 97 us -> none  [body(): lax.all_to_all(outgoing, 'sp', split_axis=0, concat_axis=0, tiled=True)]
    all_to_all x6 -> x0, starting transfers between devices: 39.8 us -> none  [the longest x1 14.3 us: body(): lax.all_to_all(value_vectors, 'sp', split_axis=2, concat_axis=1, tiled=True)]
    dot_general x8 -> x1, matrix products: 34.5 us -> 3.61 us  [body(): mixed = jnp.dot(by_tokens, weight_all, preferred_element_type=jnp.float32)]
    unnamed x4 -> x0, other arithmetic: 23.1 us -> none
    gather x2 -> x0, local copies, waits for them, and re-layouts: 13.2 us -> none  [the longest x1 7.13 us: body(): gathered = flat_rows[slot_index].reshape(tok_rows, top_count, model_width)]
    unnamed x90 -> x19, local copies, waits for them, and re-layouts: 17.4 us -> 5.18 us
  transfers between devices with their start and end apart: 7 -> 1, of which waited for: 5 -> 0; matrix products, arithmetic and copies ran while one was open for 22% -> 3% of each run, Pallas kernels for 0% -> 22%
where the time goes in v1:
time: 234 us; the launch traced here: 231 us
  Pallas kernels  205 us (88%)
  other arithmetic  10.5 us (4%)
  local copies, waits for them, and re-layouts  7.02 us (3%)
  starting transfers between devices  4.13 us (2%)
  matrix products  3.61 us (2%)
    pallas_call x1, Pallas kernels, run_experts(): pl.pallas_call(functools.partial(experts_kernel, span, chunks), out_shape...  156 us
    pallas_call x1, Pallas kernels, mix(): pl.pallas_call(functools.partial(mix_kernel, per * rows, heads, span, spr...  49.9 us
    unnamed x19, local copies, waits for them, and re-layouts  5.18 us
  transfers between devices with their start and end apart: 1, of which 0 were waited for; matrix products, arithmetic and copies ran while one was open for 3% of the time, Pallas kernels for 22%

profile of v1, /device:TPU:0, one launch (start us, length us, event | category | flops | bytes accessed | tf_op | source)
XLA Modules:
  0.0 231.0 jit_solution(4065174130622032042)
XLA Ops:
  0.0 0.8 copy.43
  1.0 0.3 convert_reduce_fusion
  1.4 0.7 add_convert_fusion.1
  2.1 0.7 reduce_sum.81
  2.8 0.7 multiply_divide_fusion
  3.6 4.1 %collective-permute-start = (f32[2,256,2]{1,2,0:T(2,128)S(1)}, f32[2,256,2]{1,2,0:T(2,128)S(1)}, u32[]{:S(2)}, u32[]{:S(2)}) collective-permute-start(f32[2,256,2]{1,2,0:T(2,128)S(1)} %pad_maximum_fusion), channel_id=1, source_target_pairs={{0,16},{4,20},{8,24},{12,28},{16,0},{20,4},{24,8},{28,12},{1,17},{... | collective-permute-start | bytes 12296 | tf_op jit(solution)/shard_map/ppermute | solution.py:417
  7.8 0.7 reduce-precision_subtract_fusion
  8.5 0.7 reshape.211.g_in
  9.3 1.2 copy-done
  10.5 1.0 copy-done.1
  11.5 1.0 copy-done.2
  12.6 1.0 copy-done.3
  13.6 49.9 %mix.1 = (bf16[256,1024]{1,0:T(8,128)(2,1)S(1)}, bf16[1024,2048]{1,0:T(8,128)(2,1)}) custom-call(bf16[256,1024]{1,0:T(8,128)(2,1)S(1)} %bitcast.55, bf16[256,1024]{1,0:T(8,128)(2,1)S(1)} %bitcast.56, bf16[256,1024]{1,0:T(8,128)(2,1)S(1)} %bitcast.57, f32[8,2,256]{2,1,0:T(2,128)S(1)} %reshape.211.g_in, bf16[1024,512]{1,0:T(8,128)(2,1)S(1)} %copy-done), custom_call_target="tpu_custom_call" | custom-call | tf_op jit(solution)/shard_map/mix/pallas_call | solution.py:198
  63.6 3.6 %multiply_reduce_fusion = (f32[256]{0:T(256)S(1)}, f32[256,2048]{1,0:T(8,128)S(1)}) fusion(bf16[256,1024]{1,0:T(8,128)(2,1)S(1)} %get-tuple-element.7, bf16[1024,2048]{1,0:T(8,128)(2,1)} %get-tuple-element.8), kind=kOutput, calls=%fused_computation.9 | convolution fusion | flops 1074790144 | bytes 6816768 | tf_op jit(solution)/shard_map/dot_general | solution.py:444
  67.2 0.6 fusion
  67.9 1.3 fusion.2.routed
  69.2 0.2 compare_reduce_fusion.1
  69.5 0.3 copy.47
  69.8 0.3 copy.45
  70.0 0.9 add_convert_fusion.pick
  70.9 0.5 fusion.5
  71.4 1.1 maximum_maximum_fusion.weigh
  72.5 155.6 %experts.1 = f32[256,2048]{1,0:T(8,128)} custom-call(bf16[256,2048]{1,0:T(8,128)(2,1)} %fusion.2.routed, bf16[2,512,256]{2,1,0:T(8,128)(2,1)} %add_convert_fusion.pick, bf16[2,2,256,512]{3,2,1,0:T(8,128)(2,1)} %maximum_maximum_fusion.weigh, bf16[2048,1024]{1,0:T(8,128)(2,1)} %bitcast.58, bf16[2048,1024]{1,0:T(8,128)(2,1)} %bitcast.59, ...), custom_call_target="tpu_custom_call" | custom-call | tf_op jit(solution)/shard_map/experts/pallas_call | solution.py:374
  228.1 2.9 %fusion.9 = bf16[1,256,2048]{2,1,0:T(8,128)(2,1)} fusion(f32[256,2048]{1,0:T(8,128)} %experts.1, bf16[256,2048]{1,0:T(8,128)(2,1)S(1)} %get-tuple-element.20, f32[2048]{0:T(1024)S(1)} %copy-done.8), kind=kLoop, calls=%fused_computation.20 | loop fusion | flops 2097152 | bytes 4202496 | tf_op jit(solution)/shard_map/broadcast_in_dim | solution.py:449
  (28 shorter events, 0.7 us)
Async XLA Ops:
  3.6 65.7 %collective-permute-start = (f32[2,256,2]{1,2,0:T(2,128)S(1)}, f32[2,256,2]{1,2,0:T(2,128)S(1)}, u32[]{:S(2)}, u32[]{:S(2)}) collective-permute-start(f32[2,256,2]{1,2,0:T(2,128)S(1)} %pad_maximum_fusion), channel_id=1, source_target_pairs={{0,16},{4,20},{8,24},{12,28},{16,0},{20,4},{24,8},{28,12},{1,17},{... | collective-permute-start | bytes 12296 | tf_op jit(solution)/shard_map/ppermute | solution.py:417
  9.3 1.2 copy-start
  10.5 1.0 copy-start.1
  11.5 1.0 copy-start.2
  12.6 1.0 copy-start.3
  63.5 3.6 %copy-start.4 = (bf16[1,256,2048]{2,1,0:T(8,128)(2,1)S(1)}, bf16[1,256,2048]{2,1,0:T(8,128)(2,1)}, u32[]{:S(2)}) copy-start(bf16[1,256,2048]{2,1,0:T(8,128)(2,1)} %param.15) | copy-start | bytes 3145732
  63.5 3.6 %copy-start.6 = (f32[2048]{0:T(1024)S(1)}, f32[2048]{0:T(1024)}, u32[]{:S(2)}) copy-start(f32[2048]{0:T(1024)} %param.21) | copy-start | bytes 24580
  67.2 0.7 copy-start.5
  67.2 0.7 copy-start.7
  72.5 155.6 %copy-start.8 = (f32[2048]{0:T(1024)S(1)}, f32[2048]{0:T(1024)}, u32[]{:S(2)}) copy-start(f32[2048]{0:T(1024)} %param.23) | copy-start | bytes 24580

commit v2 on v1

--- a/solution.py
+++ b/solution.py
@@ -49,10 +49,19 @@
         outputs.append(mixing.astype(jnp.bfloat16).reshape(block_rows, head_count * head_width))
     return jnp.concatenate(outputs, axis=0)
 
+def is_edge(me, loc, half):
+    lower = me < half
+    first = loc < half // 2
+    return jnp.logical_or(
+        jnp.logical_and(lower, first),
+        jnp.logical_and(jnp.logical_not(lower), jnp.logical_not(first)),
+    )
+
+
 def mix_kernel(
     block, heads, span, spread,
-    q_in, k_in, v_in, g_in, ow_in, tok_out, ow_out,
-    q_all, k_all, v_all, g_all, att, send, recv, back_send, back_recv, ow_send, ow_recv,
+    q_in, k_in, v_in, g_in, ow_in, facts, residual, gains, hidden_out, routed_out, others,
+    tok_out, ow_out, mixed, fact_sem, q_all, k_all, v_all, g_all, att, send, recv, back_send, back_recv, ow_send, ow_recv,
 ):
     me = lax.axis_index("sp")
     mine = lax.axis_index("dp")
@@ -68,25 +77,54 @@
 
     own_rows = pl.ds(pl.multiple_of(me * rows, rows), rows)
     pairs = ((q_in, q_all), (k_in, k_all), (v_in, v_all))
-    sends = []
-    for d in sorted(range(1, span), key=lambda d: -min(d, span - d)):
-        peer = lax.rem(me + d, span)
+    half = span // 2
+    base = (me // half) * half
+    loc = me - base
+    mirror = lax.rem(me + half, span)
+    fact_send = pltpu.make_async_remote_copy(
+        src_ref=facts, dst_ref=others, send_sem=fact_sem.at[0], recv_sem=fact_sem.at[1],
+        device_id={"sp": mirror}, device_id_type=MESH,
+    )
+    fact_send.start()
+
+    def to_peer(d, peer):
         lanes = pl.ds(pl.multiple_of(peer * width, width), width)
-        for a, (src, dst) in enumerate(pairs):
-            sends.append(
-                pltpu.make_async_remote_copy(
-                    src_ref=src.at[:, lanes], dst_ref=dst.at[own_rows, :],
-                    send_sem=send.at[a, d], recv_sem=recv.at[a, me],
-                    device_id={"sp": peer}, device_id_type=MESH,
-                )
+        copies = [
+            pltpu.make_async_remote_copy(
+                src_ref=src.at[:, lanes], dst_ref=dst.at[own_rows, :],
+                send_sem=send.at[a, d], recv_sem=recv.at[a, me],
+                device_id={"sp": peer}, device_id_type=MESH,
             )
-        sends.append(
+            for a, (src, dst) in enumerate(pairs)
+        ]
+        copies.append(
             pltpu.make_async_remote_copy(
                 src_ref=g_in.at[peer], dst_ref=g_all.at[me],
                 send_sem=send.at[3, d], recv_sem=recv.at[3, me],
                 device_id={"sp": peer}, device_id_type=MESH,
             )
         )
+        return copies
+
+    near = [copy for d in range(1, half) for copy in to_peer(d, base + lax.rem(loc + d, half))]
+    far = [
+        copy
+        for d in range(half)
+        for copy in to_peer(half + d, (half - base) + lax.rem(loc + d, half))
+    ]
+    edge = is_edge(me, loc, half)
+
+    @pl.when(edge)
+    def _():
+        for copy in near + far:
+            copy.start()
+
+    @pl.when(jnp.logical_not(edge))
+    def _():
+        for copy in far + near:
+            copy.start()
+
+    sends = near + far
     ow_lanes = pl.ds(pl.multiple_of(mine * cols, cols), cols)
     ow_sends = []
     for d in range(1, spread):
@@ -97,7 +135,7 @@
                 device_id={"dp": lax.rem(mine + d, spread)}, device_id_type=MESH,
             )
         )
-    for copy in sends + ow_sends:
+    for copy in ow_sends:
         copy.start()
     own_lanes = pl.ds(pl.multiple_of(me * width, width), width)
     for a, (src, dst) in enumerate(pairs):
@@ -179,31 +217,61 @@
         @pl.when(me != s)
         def _():
             returned(s).wait_send()
-    for copy in sends:
-        copy.wait_send()
     ow_local.wait()
     for copy in ow_sends:
         copy.wait()
-
-
-def mix(queries, keys, values, gates, out_weight, span, spread):
+    model = mixed.shape[1]
+    piece = math.gcd(512, model)
+    square = jnp.zeros((rows, 1), jnp.float32)
+    for c in range(model // piece):
+        value = jnp.dot(
+            tok_out[...], ow_out[:, pl.ds(c * piece, piece)], preferred_element_type=jnp.float32
+        )
+        mixed[:, pl.ds(c * piece, piece)] = value
+        square = square + jnp.sum(value * value, axis=1, keepdims=True)
+    inverse = lax.rsqrt(square / model + 1e-06)
+    square = jnp.zeros((rows, 1), jnp.float32)
+    for c in range(model // piece):
+        at = pl.ds(c * piece, piece)
+        value = residual[:, at].astype(jnp.float32) + mixed[:, at] * inverse * gains[pl.ds(0, 1), at]
+        value = value.astype(jnp.bfloat16)
+        hidden_out[:, at] = value
+        value = value.astype(jnp.float32)
+        square = square + jnp.sum(value * value, axis=1, keepdims=True)
+    inverse = lax.rsqrt(square / model + 1e-06)
+    for c in range(model // piece):
+        at = pl.ds(c * piece, piece)
+        value = hidden_out[:, at].astype(jnp.float32) * inverse * gains[pl.ds(1, 1), at]
+        routed_out[:, at] = value.astype(jnp.bfloat16)
+    fact_send.wait()
+    for copy in sends:
+        copy.wait_send()
+
+
+def mix(queries, keys, values, gates, out_weight, facts, residual, gains, span, spread):
     rows, full = queries.shape
     width = full // span
     heads = gates.shape[1] // span
     per = 2 if span % 2 == 0 else 1
     g = gates.T.reshape(span, heads, rows)
     vm = pl.BlockSpec(memory_space=pltpu.VMEM)
+    hbm = pl.BlockSpec(memory_space=pl.ANY)
     dma = pltpu.SemaphoreType.DMA
     wide = pltpu.VMEM((span * rows, width), jnp.bfloat16)
     return pl.pallas_call(
         functools.partial(mix_kernel, per * rows, heads, span, spread),
         out_shape=(
-            jax.ShapeDtypeStruct((rows, full), jnp.bfloat16),
-            jax.ShapeDtypeStruct((full, out_weight.shape[1] * spread), jnp.bfloat16),
+            jax.ShapeDtypeStruct(residual.shape, jnp.bfloat16),
+            jax.ShapeDtypeStruct(residual.shape, jnp.bfloat16),
+            jax.ShapeDtypeStruct(facts.shape, jnp.float32),
         ),
-        in_specs=[vm] * 5,
-        out_specs=(vm, vm),
+        in_specs=[hbm, hbm, hbm, vm, hbm, vm, vm, vm],
+        out_specs=(vm, vm, vm),
         scratch_shapes=[
+            pltpu.VMEM((rows, full), jnp.bfloat16),
+            pltpu.VMEM((full, residual.shape[1]), jnp.bfloat16),
+            pltpu.VMEM(residual.shape, jnp.float32),
+            dma((2,)),
             wide, wide, wide, pltpu.VMEM((span, heads, rows), jnp.float32), wide,
             dma((4, span)), dma((4, span)), dma((span,)), dma((span,)), dma((spread,)), dma((spread,)),
         ],
@@ -211,7 +279,7 @@
             collective_id=0, has_side_effects=True, vmem_limit_bytes=50 * 1024 * 1024
         ),
         name="mix",
-    )(queries, keys, values, g, out_weight)
+    )(queries, keys, values, g, out_weight, facts, residual, gains)
 
 
 def experts_kernel(
@@ -251,8 +319,18 @@
         copy.start()
         pending.append(copy)
 
-    for c in range(chunks):
-        begin(remote(routed.at[:, cols(c)], mir.at[:, cols(c)], mir_s.at[c], mir_r.at[c], mirror))
+    edge = is_edge(me, loc, half)
+    to_mirror = [
+        remote(routed.at[:, cols(c)], mir.at[:, cols(c)], mir_s.at[c], mir_r.at[c], mirror)
+        for c in range(chunks)
+    ]
+    pending.extend(to_mirror)
+
+    @pl.when(jnp.logical_not(edge))
+    def _():
+        for copy in to_mirror:
+            copy.start()
+
     loads = [
         pltpu.make_async_copy(src, dst, w_sem.at[i])
         for i, (src, dst) in enumerate(((gate_in, w_gate), (up_in, w_up), (down_in, w_down)))
@@ -270,6 +348,12 @@
                 chosen, routed[:, cols(c)], preferred_element_type=jnp.float32
             ).astype(jnp.bfloat16)
         begin(remote(out_own.at[p], arrived.at[0, loc], dir_s.at[d], dir_r.at[loc], base + p))
+
+    @pl.when(edge)
+    def _():
+        for copy in to_mirror:
+            copy.start()
+
     chosen = pick[0, rows_of(loc), :]
     for c in range(chunks):
         arrived[0, loc, :, cols(c)] = jnp.dot(
@@ -404,6 +488,7 @@
     tok_rows = residual.shape[1]
     width = queries.shape[2] // span
 
+    top_count = routes.shape[2]
     cap = 4 * tok_rows // span
     half = span // 2
     assigned = routes[0].reshape(-1)
@@ -413,25 +498,11 @@
     slots = (assigned * cap + ranking).reshape(routes.shape[1:]).astype(jnp.float32)
     shares = expert_share[0]
     weights = group_share[0][:, None] * shares / jnp.sum(shares, axis=1, keepdims=True)
-    facts = jnp.stack([slots, weights])
-    other = lax.ppermute(facts, "sp", [(i, (i + half) % span) for i in range(span)])
-    base = (lax.axis_index("sp") // half) * half
-    places = (base * cap + jnp.arange(half * cap, dtype=jnp.int32)).astype(jnp.float32)
-    picks, weighs = [], []
-    for both in (facts, other):
-        hit = both[0][:, :, None] == places[None, None, :]
-        picks.append(jnp.any(hit, axis=1).T.astype(jnp.bfloat16))
-        high = lax.reduce_precision(both[1], 8, 7)
-        weighs.append(
-            jnp.stack(
-                [jnp.sum(jnp.where(hit, w[:, :, None], 0.0), axis=1) for w in (high, both[1] - high)]
-            ).astype(jnp.bfloat16)
-        )
-    pick, weigh = jnp.stack(picks), jnp.stack(weighs)
-
+    facts = jnp.concatenate([slots.T, weights.T], axis=0)
     if width % 128 == 0:
-        by_tokens, weight_all = mix(
-            queries[0], key_vectors[0], value_vectors[0], gate_cache[0], out_weight, span, spread
+        hidden, routed, other = mix(
+            queries[0], key_vectors[0], value_vectors[0], gate_cache[0], out_weight, facts,
+            residual[0], jnp.stack([mix_gain, route_gain]), span, spread,
         )
     else:
         by_heads = [
@@ -441,9 +512,26 @@
         attended = attend(*(x[0] for x in by_heads))
         by_tokens = lax.all_to_all(attended[None], "sp", split_axis=1, concat_axis=2, tiled=True)[0]
         weight_all = lax.all_gather(out_weight, "dp", axis=1, tiled=True)
-    mixed = jnp.dot(by_tokens, weight_all, preferred_element_type=jnp.float32)
-    hidden = (residual[0].astype(jnp.float32) + normalize(mixed) * mix_gain).astype(jnp.bfloat16)
-    routed = (normalize(hidden.astype(jnp.float32)) * route_gain).astype(jnp.bfloat16)
+        mixed = jnp.dot(by_tokens, weight_all, preferred_element_type=jnp.float32)
+        hidden = residual[0].astype(jnp.float32) + normalize(mixed) * mix_gain
+        hidden = hidden.astype(jnp.bfloat16)
+        routed = (normalize(hidden.astype(jnp.float32)) * route_gain).astype(jnp.bfloat16)
+        other = lax.ppermute(facts, "sp", [(i, (i + half) % span) for i in range(span)])
+    base = (lax.axis_index("sp") // half) * half
+    places = (base * cap + jnp.arange(half * cap, dtype=jnp.int32)).astype(jnp.float32)
+    picks, weighs = [], []
+    for both in (facts, other):
+        slot, share = both[:top_count], both[top_count:]
+        picks.append(jnp.any(slot[:, None, :] == places[None, :, None], axis=0).astype(jnp.bfloat16))
+        hit = slot[:, :, None] == places[None, None, :]
+        high = lax.reduce_precision(share, 8, 7)
+        weighs.append(
+            jnp.stack(
+                [jnp.sum(jnp.where(hit, w[:, :, None], 0.0), axis=0) for w in (high, share - high)]
+            ).astype(jnp.bfloat16)
+        )
+    pick, weigh = jnp.stack(picks), jnp.stack(weighs)
+
     combined = run_experts(routed, pick, weigh, gate_proj[0], up_proj[0], down_proj[0], span, cap)
     layer_out = (hidden.astype(jnp.float32) + combined * out_gain).astype(jnp.bfloat16)
     return layer_out[None]

time: 234 us -> 227 us (0.970)
  Pallas kernels: 205 us -> 210 us
  starting transfers between devices: 4.13 us -> 0 us
  matrix products: 3.61 us -> 0 us
    pallas_call x1, Pallas kernels: 49.9 us -> 61.7 us  [mix(): pl.pallas_call(functools.partial(mix_kernel, per * rows, heads, span, spr...]
    pallas_call x1, Pallas kernels: 156 us -> 148 us  [run_experts(): pl.pallas_call(functools.partial(experts_kernel, span, chunks), out_shape...]
    ppermute x1 -> x0, starting transfers between devices: 4.13 us -> none  [body(): lax.ppermute(facts, 'sp', [(i, (i + half) % span) for i in range(span)])]
    dot_general x1 -> x0, matrix products: 3.61 us -> none  [body(): mixed = jnp.dot(by_tokens, weight_all, preferred_element_type=jnp.float32)]
    unnamed x19 -> x11, local copies, waits for them, and re-layouts: 5.18 us -> 4.9 us
  transfers between devices with their start and end apart: 1 -> 0, of which waited for: 0 -> 0; matrix products, arithmetic and copies ran while one was open for 3% -> 0% of each run, Pallas kernels for 22% -> 0%
where the time goes in v2:
time: 227 us; the launch traced here: 225 us
  Pallas kernels  210 us (93%)
  other arithmetic  8.66 us (4%)
  local copies, waits for them, and re-layouts  5.99 us (3%)
    pallas_call x1, Pallas kernels, run_experts(): pl.pallas_call(functools.partial(experts_kernel, span, chunks), out_shape...  148 us
    pallas_call x1, Pallas kernels, mix(): pl.pallas_call(functools.partial(mix_kernel, per * rows, heads, span, spr...  61.7 us
    unnamed x11, local copies, waits for them, and re-layouts  4.9 us

profile of v2, /device:TPU:0, one launch (start us, length us, event | category | flops | bytes accessed | tf_op | source)
XLA Modules:
  0.0 224.9 jit_solution(16103874566473239489)
XLA Ops:
  0.0 0.7 reduce_sum.58
  0.7 0.7 reduce-precision_subtract_fusion
  1.4 0.7 reshape.115.g_in
  2.1 0.7 pad_maximum_fusion.gains
  2.9 0.8 copy.18
  3.7 0.1 eq.28
  3.8 0.3 convert_reduce_fusion
  4.1 0.1 reduce_sum.57
  4.3 0.1 copy.19
  4.3 0.7 fusion.9
  5.0 0.0 copy-start.1
  5.1 1.0 copy-done.1
  6.1 1.0 copy-done.2
  7.1 1.0 copy-done.3
  8.2 61.7 %mix.1 = (bf16[256,2048]{1,0:T(8,128)(2,1)S(1)}, bf16[256,2048]{1,0:T(8,128)(2,1)S(1)}, f32[4,256]{1,0:T(4,128)S(1)}) custom-call(bf16[256,1024]{1,0:T(8,128)(2,1)S(1)} %bitcast.47, bf16[256,1024]{1,0:T(8,128)(2,1)S(1)} %bitcast.48, bf16[256,1024]{1,0:T(8,128)(2,1)S(1)} %bitcast.49, f32[8,2,256]{2,1,0:T(2,128)S(1)} %reshape.115.g_in, ...), custom_call_target="tpu_custom_call" | custom-call | tf_op jit(solution)/shard_map/mix/pallas_call | solution.py:261
  69.9 0.0 copy-start
  69.9 1.0 copy-done
  70.8 0.2 compare_reduce_fusion.1
  71.1 0.9 add_convert_fusion.1.pick
  72.0 0.5 fusion
  72.4 1.1 maximum_maximum_fusion.weigh
  73.5 148.5 %experts.1 = f32[256,2048]{1,0:T(8,128)} custom-call(bf16[256,2048]{1,0:T(8,128)(2,1)} %copy-done, bf16[2,512,256]{2,1,0:T(8,128)(2,1)} %add_convert_fusion.1.pick, bf16[2,2,256,512]{3,2,1,0:T(8,128)(2,1)} %maximum_maximum_fusion.weigh, bf16[2048,1024]{1,0:T(8,128)(2,1)} %bitcast.50, bf16[2048,1024]{1,0:T(8,128)(2,1)} %bitcast.51, bf16[1024,2048]{1,0:T(8,128)(2,1)} %bitcast.52), custom_call_target="tpu_custom_call" | custom-call | tf_op jit(solution)/shard_map/experts/pallas_call | solution.py:458
  222.0 0.0 copy-done.4
  222.0 2.9 %fusion.4 = bf16[1,256,2048]{2,1,0:T(8,128)(2,1)} fusion(f32[256,2048]{1,0:T(8,128)} %experts.1, bf16[256,2048]{1,0:T(8,128)(2,1)S(1)} %get-tuple-element.8, f32[2048]{0:T(1024)S(1)} %copy-done.4), kind=kLoop, calls=%fused_computation.9 | loop fusion | flops 2097152 | bytes 4202496 | tf_op jit(solution)/shard_map/broadcast_in_dim | solution.py:537
  (7 shorter events, 0.0 us)
Async XLA Ops:
  5.0 1.0 copy-start.1
  6.1 1.0 copy-start.2
  7.1 1.0 copy-start.3
  69.9 1.0 copy-start
  73.5 148.5 %copy-start.4 = (f32[2048]{0:T(1024)S(1)}, f32[2048]{0:T(1024)}, u32[]{:S(2)}) copy-start(f32[2048]{0:T(1024)} %param.23) | copy-start | bytes 24580
